TPU v7x, 512 devices: a whole 4x8x8 slice. The times are simulated.
512 devices in a mesh: ep: 128 (over z, y, core), tp: 4 (over x).
Axes of the slice: x: 4, y: 8, z: 8, core: 2. Of those that a mesh axis runs over, the one named last changes fastest.
Arguments:
- tokens: bfloat16 [16384, 2048], P('ep'), may hold values from -6 to 6
- norm_gain: float32 [2048], replicated, may hold values from 0.1 to 1.9
- routes: int32 [16384, 2], P('ep'), may hold values from 0 to 127, all different within a row; in each aligned block of 128 rows (0 to 127, 128 to 255, ...) at most 3 rows name the same one
- group_prob: float32 [16384], P('ep'), may hold values from 0.2 to 1
- expert_logits: float32 [16384, 2], P('ep'), may hold values from -6 to 6
- gate_weight: bfloat16 [128, 2048, 384], P('ep', None, 'tp'), may hold values from -0.125 to 0.125
- up_weight: bfloat16 [128, 2048, 384], P('ep', None, 'tp'), may hold values from -0.125 to 0.125
- down_matrix: bfloat16 [128, 384, 2048], P('ep', 'tp'), may hold values from -0.3125 to 0.3125
Outputs:
- combined: bfloat16 [16384, 2048], P('ep', 'tp')
Inputs may be any that keep to these rules, and one draw needn't show every extreme that they name: `routes`: each row names 2 different experts. Among the 128 tokens of one index of ep at most 3 rows name one expert, and in every draw some expert is named by exactly 3 of them.
All inputs are finite; a program needn't handle non-finite values.
Results may differ from a plain program's by a relative error of at most 0.013.
Values may be sent and summed in bfloat16 or wider, within the bound.
A program may use at most 64 MiB of HBM per device.

v0:
```python
import jax
import jax.numpy as jnp
from jax import lax
from jax.sharding import PartitionSpec as P


def in_order(parts, dim):
    lengths = list(parts.shape[1:])
    lengths[dim] *= parts.shape[0]
    return jnp.moveaxis(parts, 0, dim).reshape(lengths)


def sent_to_all(shard, axis):
    copies = jnp.broadcast_to(shard, (lax.axis_size(axis), *shard.shape))
    return lax.all_to_all(copies, axis, split_axis=0, concat_axis=0, tiled=True)


def gathered_copies(shard, axis, dim):
    return in_order(sent_to_all(shard, axis), dim)


def hidden_part(buffer, gate_weight, up_weight):
    local_count = gate_weight.shape[0]
    grouped = buffer.reshape(
        buffer.shape[0] // local_count, local_count, buffer.shape[1], buffer.shape[2]
    )
    gate_proj = jnp.einsum(
        "sknd,kdf->sknf", grouped, gate_weight, preferred_element_type=jnp.float32
    )
    up_proj = jnp.einsum("sknd,kdf->sknf", grouped, up_weight, preferred_element_type=jnp.float32)
    hidden_state = (jax.nn.silu(gate_proj) * up_proj).astype(jnp.bfloat16)
    return hidden_state.reshape(buffer.shape[0], buffer.shape[1], hidden_state.shape[3])


def down_blocks(hidden_full, down_cols, block_count):
    local_count = down_cols.shape[0]
    width = hidden_full.shape[2] // block_count
    grouped = hidden_full.reshape(
        hidden_full.shape[0] // local_count, local_count, hidden_full.shape[1], block_count, width
    )
    columns = down_cols.reshape(local_count, block_count, width, down_cols.shape[2])
    block_list = jnp.einsum(
        "sknrf,krfd->sknrd", grouped, columns, preferred_element_type=jnp.float32
    ).astype(jnp.bfloat16)
    summed = jnp.sum(block_list.astype(jnp.float32), 3).astype(jnp.bfloat16)
    return summed.reshape(hidden_full.shape[0], hidden_full.shape[1], down_cols.shape[2])


def body(tokens, norm_gain, routes, group_prob, expert_logits, gate_weight, up_weight, down_matrix):
    tok_rows, model_width = tokens.shape
    top_count = routes.shape[1]
    experts = gate_weight.shape[0] * lax.axis_size("ep")
    capacity = 3 * top_count * tok_rows // (2 * experts)
    block_count = lax.axis_size("tp")
    down_cols = lax.all_to_all(down_matrix, "tp", split_axis=2, concat_axis=1, tiled=True)
    values = tokens.astype(jnp.float32)
    normed = (
        values * lax.rsqrt(jnp.mean(values * values, -1, keepdims=True) + 1e-06) * norm_gain
    ).astype(jnp.bfloat16)
    flat_ids = routes.reshape(-1)
    onehot = (flat_ids[:, None] == jnp.arange(experts, dtype=jnp.int32)[None, :]).astype(jnp.int32)
    earlier = jnp.cumsum(onehot, 0) - onehot
    slot_index = jnp.sum(earlier * onehot, 1)
    target = flat_ids * capacity + slot_index
    owners = jnp.arange(tok_rows * top_count, dtype=jnp.int32) // top_count
    outgoing = (
        jnp.zeros((experts * capacity, model_width), jnp.bfloat16).at[target].set(normed[owners])
    )
    outgoing = outgoing.reshape(experts, capacity, model_width)
    feature_share = model_width // block_count
    my_features = lax.dynamic_slice_in_dim(
        outgoing, lax.axis_index("tp") * feature_share, feature_share, 2
    )
    arrived = lax.all_to_all(my_features, "ep", split_axis=0, concat_axis=0, tiled=True)
    full_rows = gathered_copies(arrived, "tp", 2)
    hidden_state = hidden_part(full_rows, gate_weight, up_weight)
    hidden_full = gathered_copies(hidden_state, "tp", 2)
    summed = down_blocks(hidden_full, down_cols, block_count)
    returned = lax.all_to_all(summed, "ep", split_axis=0, concat_axis=0, tiled=True)
    flat_back = returned.reshape(experts * capacity, returned.shape[2])
    weights = group_prob[:, None] * jax.nn.softmax(expert_logits, axis=-1)
    picked = flat_back[target].reshape(tok_rows, top_count, flat_back.shape[1]).astype(jnp.float32)
    combined = jnp.sum(picked * weights[:, :, None], 1).astype(jnp.bfloat16)
    return combined


def solution(mesh):
    return jax.shard_map(
        body,
        mesh=mesh,
        in_specs=(
            P("ep", None),
            P(),
            P("ep", None),
            P("ep"),
            P("ep", None),
            P("ep", None, "tp"),
            P("ep", None, "tp"),
            P("ep", "tp", None),
        ),
        out_specs=P("ep", "tp"),
        check_vma=False,
    )
```

profile of v0, /device:TPU:1, one launch (start us, length us, event | category | flops | bytes accessed | tf_op | source)
XLA Modules:
  0.0 136.8 jit_solution(1834693873175598776)
XLA Ops:
  0.0 0.9 copy.34
  1.2 0.7 broadcast_multiply_fusion
  2.5 1.2 fusion.4
  4.2 5.9 %scatter_custom_fusion = bf16[384,2048]{1,0:T(8,128)(2,1)S(1)} fusion(s32[256]{0:T(256)S(1)} %bitcast.72, bf16[128,2048]{1,0:T(8,128)(2,1)S(1)} %fusion.6, s32[1024]{0:T(1024)S(1)} %pad_clamp_fusion.1, bf16[]{:T(256)} %constant.18.clone.1), kind=kCustom, calls=%fused_computation.15 | custom fusion | bytes 1572866 | tf_op jit(solution)/shard_map/scatter | solution.py:67
  10.1 2.3 %reshape.142 = bf16[128,3,2048]{2,1,0:T(4,128)(2,1)} reshape(bf16[384,2048]{1,0:T(8,128)(2,1)S(1)} %scatter_custom_fusion) | data formatting | bytes 3145728 | tf_op jit(solution)/shard_map/reshape | solution.py:69
  12.5 2.1 %constant_dynamic-slice_fusion = bf16[128,3,512]{2,1,0:T(4,128)(2,1)} fusion(bf16[128,3,2048]{2,1,0:T(4,128)(2,1)} %reshape.142, s32[]{:T(128)S(6)} %select_n.39), kind=kLoop, calls=%fused_computation.46 | loop fusion | bytes 786436 | tf_op jit(solution)/shard_map/dynamic_slice | solution.py:71
  14.5 18.4 %all-to-all-start.1 = ((bf16[128,3,512]{2,1,0:T(4,128)(2,1)}), bf16[128,3,512]{2,1,0:T(4,128)(2,1)S(1)}, u32[]{:S(2)}, u32[]{:S(2)}) async-start(bf16[128,3,512]{2,1,0:T(4,128)(2,1)} %constant_dynamic-slice_fusion), calls=%async_computation.1 | async-start | bytes 1048576 | tf_op jit(solution)/shard_map/all_to_all | solution.py:74
  33.0 0.8 copy.28
  33.7 0.5 broadcast.137
  34.2 11.5 %reduce.4 = bf16[2048,96]{1,0:T(8,128)(2,1)S(1)} reduce(bf16[2048,1,96]{2,1,0:T(2,128)(2,1)S(1)} %bitcast.65, bf16[]{:T(256)} %broadcast.137), dimensions={1}, to_apply=%bitcast.53.reduce_sub_computation | reduce | bytes 786434
  45.8 1.6 %reshape.182 = bf16[4,2,24576]{2,1,0:T(2,128)(2,1)} reshape(bf16[2048,96]{1,0:T(8,128)(2,1)S(1)} %reduce.4) | data formatting | bytes 786432
  47.3 6.2 %all-to-all-done.1 = bf16[128,3,512]{2,1,0:T(4,128)(2,1)S(1)} async-done(((bf16[128,3,512]{2,1,0:T(4,128)(2,1)}), bf16[128,3,512]{2,1,0:T(4,128)(2,1)S(1)}, u32[]{:S(2)}, u32[]{:S(2)}) %all-to-all-start.1) | async-done | bytes 393248 | tf_op jit(solution)/shard_map/all_to_all | solution.py:74
  53.5 4.0 %all-to-all-start = ((bf16[4,2,24576]{2,1,0:T(2,128)(2,1)}), bf16[4,2,24576]{2,1,0:T(2,128)(2,1)S(1)}, u32[]{:S(2)}, u32[]{:S(2)}) async-start(bf16[4,2,24576]{2,1,0:T(2,128)(2,1)} %reshape.182), calls=%async_computation | async-start | bytes 786432 | tf_op jit(solution)/shard_map/all_to_all | solution.py:55
  57.6 8.1 %all-to-all-done = bf16[4,2,24576]{2,1,0:T(2,128)(2,1)S(1)} async-done(((bf16[4,2,24576]{2,1,0:T(2,128)(2,1)}), bf16[4,2,24576]{2,1,0:T(2,128)(2,1)S(1)}, u32[]{:S(2)}, u32[]{:S(2)}) %all-to-all-start) | async-done | bytes 393248 | tf_op jit(solution)/shard_map/all_to_all | solution.py:55
  65.7 1.3 broadcast_in_dim.7
  67.0 3.6 %all-to-all-start.2 = ((bf16[4,128,3,512]{3,1,2,0:T(8,128)(2,1)}), bf16[4,128,3,512]{3,1,2,0:T(8,128)(2,1)S(1)}, u32[]{:S(2)}, u32[]{:S(2)}) async-start(bf16[4,128,3,512]{3,1,2,0:T(8,128)(2,1)} %broadcast_in_dim.7), calls=%async_computation.2 | async-start | bytes 3145728 | tf_op jit(solution)/shard_map/all_to_all | solution.py:15
  70.5 0.8 reshape.183
  71.3 19.1 %all-to-all-done.2 = bf16[4,128,3,512]{3,1,2,0:T(8,128)(2,1)S(1)} async-done(((bf16[4,128,3,512]{3,1,2,0:T(8,128)(2,1)}), bf16[4,128,3,512]{3,1,2,0:T(8,128)(2,1)S(1)}, u32[]{:S(2)}, u32[]{:S(2)}) %all-to-all-start.2) | async-done | bytes 1572896 | tf_op jit(solution)/shard_map/all_to_all | solution.py:15
  90.6 0.6 convolution_bitcast_fusion.1
  91.2 0.4 copy-done.6
  91.6 0.6 fusion.3
  92.2 0.7 broadcast_in_dim.8
  93.0 3.5 %all-to-all-start.3 = ((bf16[4,128,3,96]{1,3,2,0:T(8,128)(2,1)}), bf16[4,128,3,96]{1,3,2,0:T(8,128)(2,1)S(1)}, u32[]{:S(2)}, u32[]{:S(2)}) async-start(bf16[4,128,3,96]{1,3,2,0:T(8,128)(2,1)} %broadcast_in_dim.8), calls=%async_computation.3 | async-start | bytes 589824 | tf_op jit(solution)/shard_map/all_to_all | solution.py:15
  96.4 1.1 fusion.19
  98.1 4.0 %all-to-all-done.3 = bf16[4,128,3,96]{1,3,2,0:T(8,128)(2,1)S(1)} async-done(((bf16[4,128,3,96]{1,3,2,0:T(8,128)(2,1)}), bf16[4,128,3,96]{1,3,2,0:T(8,128)(2,1)S(1)}, u32[]{:S(2)}, u32[]{:S(2)}) %all-to-all-start.3) | async-done | bytes 294944 | tf_op jit(solution)/shard_map/all_to_all | solution.py:15
  102.1 0.6 fusion
  102.7 1.2 copy.40
  103.9 9.1 %all-to-all-start.4 = ((bf16[128,3,512]{2,1,0:T(4,128)(2,1)}), bf16[128,3,512]{2,1,0:T(4,128)(2,1)S(1)}, u32[]{:S(2)}, u32[]{:S(2)}) async-start(bf16[128,3,512]{2,1,0:T(4,128)(2,1)} %copy.40), calls=%async_computation.4 | async-start | bytes 1048576 | tf_op jit(solution)/shard_map/all_to_all | solution.py:79
  113.2 20.4 %all-to-all-done.4 = bf16[128,3,512]{2,1,0:T(4,128)(2,1)S(1)} async-done(((bf16[128,3,512]{2,1,0:T(4,128)(2,1)}), bf16[128,3,512]{2,1,0:T(4,128)(2,1)S(1)}, u32[]{:S(2)}, u32[]{:S(2)}) %all-to-all-start.4) | async-done | bytes 393248 | tf_op jit(solution)/shard_map/all_to_all | solution.py:79
  133.9 1.2 gather_fusion
  135.1 0.3 reshape.148
  135.4 1.4 multiply_reduce_fusion
  (44 shorter events, 2.6 us)
Async XLA Ops:
  0.0 90.6 %copy-start = (bf16[1,2048,96]{1,2,0:T(8,128)(2,1)S(1)}, bf16[1,2048,96]{1,2,0:T(8,128)(2,1)}, u32[]{:S(2)}) copy-start(bf16[1,2048,96]{1,2,0:T(8,128)(2,1)} %param.13) | copy-start | bytes 1179652
  0.0 4.0 %copy-start.1 = (bf16[128,2048]{1,0:T(8,128)(2,1)S(1)}, bf16[128,2048]{1,0:T(8,128)(2,1)}, u32[]{:S(2)}) copy-start(bf16[128,2048]{1,0:T(8,128)(2,1)} %param.8) | copy-start | bytes 1572868
  0.0 4.0 %copy-start.4 = (f32[2048]{0:T(1024)S(1)}, f32[2048]{0:T(1024)}, u32[]{:S(2)}) copy-start(f32[2048]{0:T(1024)} %param.9) | copy-start | bytes 24580
  12.5 20.5 %copy-start.2 = (bf16[1,96,2048]{2,1,0:T(8,128)(2,1)S(1)}, bf16[1,96,2048]{2,1,0:T(8,128)(2,1)}, u32[]{:S(2)}) copy-start(bf16[1,96,2048]{2,1,0:T(8,128)(2,1)} %param.15) | copy-start | bytes 1179652
  14.5 39.0 %all-to-all-start.1 = ((bf16[128,3,512]{2,1,0:T(4,128)(2,1)}), bf16[128,3,512]{2,1,0:T(4,128)(2,1)S(1)}, u32[]{:S(2)}, u32[]{:S(2)}) async-start(bf16[128,3,512]{2,1,0:T(4,128)(2,1)} %constant_dynamic-slice_fusion), calls=%async_computation.1 | async-start | bytes 1048576 | tf_op jit(solution)/shard_map/all_to_all | solution.py:74
  53.5 12.2 %all-to-all-start = ((bf16[4,2,24576]{2,1,0:T(2,128)(2,1)}), bf16[4,2,24576]{2,1,0:T(2,128)(2,1)S(1)}, u32[]{:S(2)}, u32[]{:S(2)}) async-start(bf16[4,2,24576]{2,1,0:T(2,128)(2,1)} %reshape.182), calls=%async_computation | async-start | bytes 786432 | tf_op jit(solution)/shard_map/all_to_all | solution.py:55
  67.0 23.5 %all-to-all-start.2 = ((bf16[4,128,3,512]{3,1,2,0:T(8,128)(2,1)}), bf16[4,128,3,512]{3,1,2,0:T(8,128)(2,1)S(1)}, u32[]{:S(2)}, u32[]{:S(2)}) async-start(bf16[4,128,3,512]{3,1,2,0:T(8,128)(2,1)} %broadcast_in_dim.7), calls=%async_computation.2 | async-start | bytes 3145728 | tf_op jit(solution)/shard_map/all_to_all | solution.py:15
  90.6 1.0 copy-start.6
  93.0 9.1 %all-to-all-start.3 = ((bf16[4,128,3,96]{1,3,2,0:T(8,128)(2,1)}), bf16[4,128,3,96]{1,3,2,0:T(8,128)(2,1)S(1)}, u32[]{:S(2)}, u32[]{:S(2)}) async-start(bf16[4,128,3,96]{1,3,2,0:T(8,128)(2,1)} %broadcast_in_dim.8), calls=%async_computation.3 | async-start | bytes 589824 | tf_op jit(solution)/shard_map/all_to_all | solution.py:15
  102.1 11.0 %copy-start.3 = (f32[128,2]{0,1:T(2,128)S(1)}, f32[128,2]{0,1:T(2,128)}, u32[]{:S(2)}) copy-start(f32[128,2]{0,1:T(2,128)} %param.12) | copy-start | bytes 3076
  102.1 11.0 %copy-start.5 = (f32[128]{0:T(128)S(1)}, f32[128]{0:T(128)}, u32[]{:S(2)}) copy-start(f32[128]{0:T(128)} %param.11) | copy-start | bytes 1540
  103.9 29.7 %all-to-all-start.4 = ((bf16[128,3,512]{2,1,0:T(4,128)(2,1)}), bf16[128,3,512]{2,1,0:T(4,128)(2,1)S(1)}, u32[]{:S(2)}, u32[]{:S(2)}) async-start(bf16[128,3,512]{2,1,0:T(4,128)(2,1)} %copy.40), calls=%async_computation.4 | async-start | bytes 1048576 | tf_op jit(solution)/shard_map/all_to_all | solution.py:79
where the time goes:
time: 137 us
  waiting for transfers between devices  57.7 us (42%)
  starting transfers between devices  38.6 us (28%)
  local copies, waits for them, and re-layouts  22.9 us (17%)
  other arithmetic  15.6 us (11%)
  matrix products  1.82 us (1%)
    all_to_all x2, waiting for transfers between devices, sent_to_all(): return lax.all_to_all(copies, axis, split_axis=0, concat_axis=0, tiled=True)  23.1 us
    all_to_all x1, waiting for transfers between devices, body(): lax.all_to_all(summed, 'ep', split_axis=0, concat_axis=0, tiled=True)  20.4 us
    all_to_all x1, starting transfers between devices, body(): lax.all_to_all(my_features, 'ep', split_axis=0, concat_axis=0, tiled=True)  18.4 us
    unnamed x1, other arithmetic  11.5 us
    all_to_all x1, starting transfers between devices, body(): lax.all_to_all(summed, 'ep', split_axis=0, concat_axis=0, tiled=True)  9.14 us
    all_to_all x1, waiting for transfers between devices, body(): lax.all_to_all(down_matrix, 'tp', split_axis=2, concat_axis=1, tiled=True)  8.05 us
    all_to_all x2, starting transfers between devices, sent_to_all(): return lax.all_to_all(copies, axis, split_axis=0, concat_axis=0, tiled=True)  7.01 us
    all_to_all x1, waiting for transfers between devices, body(): lax.all_to_all(my_features, 'ep', split_axis=0, concat_axis=0, tiled=True)  6.16 us
  transfers between devices with their start and end apart: 5, of which 5 were waited for; matrix products, arithmetic and copies ran while one was open for 12% of the time, Pallas kernels for 0%

commit v1 on v0

v1 whole, which is shorter than its diff:
```python
import functools

import jax
import jax.numpy as jnp
from jax import lax
from jax.experimental import pallas as pl
from jax.experimental.pallas import tpu as pltpu
from jax.sharding import PartitionSpec as P

MESH = pl.DeviceIdType.MESH
CAP = 3
CORES = 2
F32, BF16 = jnp.float32, jnp.bfloat16


def quotient(values, divisor):
    return lax.shift_right_logical(values * ((65535 + divisor) // divisor), 16)


def far_first(n):
    return sorted(range(1, n), key=lambda d: -min(d, n - d))


def dot(a, b):
    return jnp.dot(a, b, preferred_element_type=F32)


def dot_nt(a, b):
    return lax.dot_general(a, b, (((1,), (1,)), ((), ())), preferred_element_type=F32)


def kernel(
    nz, nyc, ntp,
    tokens, gain, routes, prob, logits, gate, up, down,
    out,
    wg, dn, oa, ob, a1, b1, a1p, b1p, a2, b2, ps, pr, hid, ra, rb, ra1, rb1, ra1p, rb1p, ra2, rb2,
    lsem, wss, wrs, s1s, s1r, s2s, s2r, pss, prs, hss, hrs, s3s, s3r, s4s, s4r, us, ur,
):
    ny = nyc // CORES
    ep, tp = lax.axis_index("ep"), lax.axis_index("tp")
    z, yc = lax.div(ep, nyc), lax.rem(ep, nyc)
    y, core = lax.div(yc, CORES), lax.rem(yc, CORES)
    width = tokens.shape[1]
    share = width // ntp
    half = share // 2
    ff = gate.shape[0]
    experts = nz * nyc
    slots = experts * CAP
    tok = tokens.shape[0]

    z_steps = far_first(nz)
    yc_steps = [(dy, dc) for dy in [*far_first(ny), 0] for dc in range(CORES) if dy or dc]
    x_steps = far_first(ntp)

    def z_to(d):
        return lax.rem(z + d, nz)

    def yc_to(dy, dc):
        return lax.rem(y + dy, ny) * CORES + lax.rem(core + dc, CORES)

    def x_to(d):
        return lax.rem(tp + d, ntp)

    z_peers = [((z_to(d) * nyc + yc, tp), z_to(d), z_to(nz - d), d) for d in z_steps]
    yc_peers = [
        ((z * nyc + yc_to(dy, dc), tp), yc_to(dy, dc), yc_to(ny - dy, dc), dy * CORES + dc)
        for dy, dc in yc_steps
    ]
    x_peers = [((ep, x_to(d)), x_to(d), x_to(ntp - d), d) for d in x_steps]

    barrier = pltpu.get_barrier_semaphore()
    for device, *_ in [*z_peers, *yc_peers, *x_peers]:
        pl.semaphore_signal(barrier, inc=1, device_id=device, device_id_type=MESH)

    pending = []

    def send(src, dst, ssem, rsem, device):
        copy = pltpu.make_async_remote_copy(
            src_ref=src, dst_ref=dst, send_sem=ssem, recv_sem=rsem, device_id=device, device_id_type=MESH
        )
        copy.start()
        pending.append(copy)

    def arrived(dst, ssem, rsem, device):
        pltpu.make_async_remote_copy(
            src_ref=dst, dst_ref=dst, send_sem=ssem, recv_sem=rsem, device_id=device, device_id_type=MESH
        ).wait_recv()

    def exchange(src, dst, peers, mine, ssem, rsem):
        for device, there, _, k in peers:
            send(src.at[there], dst.at[mine], ssem.at[k], rsem.at[k], device)

    def await_all(dst, peers, ssem, rsem):
        for device, _, source, k in peers:
            arrived(dst.at[source], ssem.at[k], rsem.at[k], device)

    def columns(j):
        return pl.ds(pl.multiple_of(j * share, share), share)

    local = [
        pltpu.make_async_copy(gate.at[:, columns(tp)], wg.at[tp, pl.ds(0, ff)], lsem.at[0]),
        pltpu.make_async_copy(up.at[:, columns(tp)], wg.at[tp, pl.ds(ff, ff)], lsem.at[1]),
        pltpu.make_async_copy(down.at[:, columns(tp)], dn.at[tp], lsem.at[2]),
    ]
    for copy in local:
        copy.start()

    r0, r1 = routes[0:1, :], routes[1:2, :]
    ids = lax.broadcasted_iota(jnp.int32, (experts, tok), 0)
    e0, e1 = (ids == r0).astype(F32), (ids == r1).astype(F32)
    before = (
        lax.broadcasted_iota(jnp.int32, (tok, tok), 0) < lax.broadcasted_iota(jnp.int32, (tok, tok), 1)
    ).astype(BF16)
    earlier = dot((e0 + e1).astype(BF16), before)
    c0 = jnp.sum(earlier * e0, 0, keepdims=True).astype(jnp.int32)
    c1 = jnp.sum(earlier * e1, 0, keepdims=True).astype(jnp.int32)

    def by_z(r, c):
        return r * CAP + c

    def by_yc(r, c):
        rz = quotient(r, nyc)
        return ((r - rz * nyc) * nz + rz) * CAP + c

    rows = lax.broadcasted_iota(jnp.int32, (slots, tok), 0)
    at_a0, at_a1 = rows == by_z(r0, c0), rows == by_z(r1, c1)
    at_b0, at_b1 = rows == by_yc(r0, c0), rows == by_yc(r1, c1)

    values = tokens[...].astype(F32)
    scale = lax.rsqrt(jnp.sum(values * values, -1, keepdims=True) * (1.0 / width) + 1e-06)
    normed = (tokens[:, columns(tp)].astype(F32) * scale * gain[:, columns(tp)]).astype(BF16)

    oa[...] = dot((at_a0 | at_a1).astype(BF16), normed[:, :half]).astype(BF16).reshape(oa.shape)
    ob[...] = dot((at_b0 | at_b1).astype(BF16), normed[:, half:]).astype(BF16).reshape(ob.shape)

    pl.semaphore_wait(barrier, len(z_peers) + len(yc_peers) + len(x_peers))

    exchange(oa, a1, z_peers, z, s1s, s1r)
    exchange(ob, b1, yc_peers, yc, s2s, s2r)
    for device, there, _, d in x_peers:
        send(gate.at[:, columns(there)], wg.at[tp, pl.ds(0, ff)], wss.at[0, d], wrs.at[0, d], device)
        send(up.at[:, columns(there)], wg.at[tp, pl.ds(ff, ff)], wss.at[1, d], wrs.at[1, d], device)
    for device, there, _, d in x_peers:
        send(down.at[:, columns(there)], dn.at[tp], wss.at[2, d], wrs.at[2, d], device)
    a1[z] = oa[z]
    b1[yc] = ob[yc]

    top = jnp.maximum(logits[0:1, :], logits[1:2, :])
    x0, x1 = jnp.exp(logits[0:1, :] - top), jnp.exp(logits[1:2, :] - top)
    w0, w1 = prob[...] * (x0 / (x0 + x1)), prob[...] * (x1 / (x0 + x1))
    zero = jnp.zeros((slots, tok), F32)
    wa = (jnp.where(at_a0, w0, zero) + jnp.where(at_a1, w1, zero)).T
    wb = (jnp.where(at_b0, w0, zero) + jnp.where(at_b1, w1, zero)).T
    wa_hi, wb_hi = wa.astype(BF16), wb.astype(BF16)
    wa_lo, wb_lo = (wa - wa_hi.astype(F32)).astype(BF16), (wb - wb_hi.astype(F32)).astype(BF16)

    to = lax.broadcasted_iota(jnp.int32, (slots, slots), 0)
    of = lax.broadcasted_iota(jnp.int32, (slots, slots), 1)

    def reorder(outer, inner):
        i = quotient(to, inner * CAP)
        rest = to - i * (inner * CAP)
        j = quotient(rest, CAP)
        return (of == (j * outer + i) * CAP + (rest - j * CAP)).astype(BF16)

    to_yz, to_zy = reorder(nyc, nz), reorder(nz, nyc)
    same = (of == to).astype(BF16)

    await_all(a1, z_peers, s1s, s1r)
    a1p[...] = dot(to_yz, a1[...].reshape(slots, half)).astype(BF16).reshape(a1p.shape)
    exchange(a1p, a2, yc_peers, yc, s3s.at[0], s3r.at[0])
    a2[yc] = a1p[yc]
    await_all(b1, yc_peers, s2s, s2r)
    b1p[...] = dot(to_zy, b1[...].reshape(slots, half)).astype(BF16).reshape(b1p.shape)
    exchange(b1p, b2, z_peers, z, s4s.at[0], s4r.at[0])
    b2[z] = b1p[z]

    for copy in local:
        copy.wait()
    for device, _, source, d in x_peers:
        arrived(wg.at[source, pl.ds(0, ff)], wss.at[0, d], wrs.at[0, d], device)
        arrived(wg.at[source, pl.ds(ff, ff)], wss.at[1, d], wrs.at[1, d], device)

    await_all(a2, yc_peers, s3s.at[0], s3r.at[0])
    await_all(b2, z_peers, s4s.at[0], s4r.at[0])
    xa = a2[...].reshape(slots, half)
    xb = dot(to_yz, b2[...].reshape(slots, half)).astype(BF16)

    def partial(j):
        return dot_nt(wg[j, :, :half], xa) + dot_nt(wg[j, :, half:], xb)

    for device, there, _, d in x_peers:
        ps[d] = partial(there).astype(BF16)
        send(ps.at[d], pr.at[d], pss.at[d], prs.at[d], device)
    total = partial(tp)
    for device, _, _, d in x_peers:
        arrived(pr.at[d], pss.at[d], prs.at[d], device)
        total = total + pr[d].astype(F32)
    g, u = total[:ff], total[ff:]
    hid[tp] = (g / (1.0 + jnp.exp(-g)) * u).astype(BF16)
    for device, _, _, d in x_peers:
        send(hid.at[tp], hid.at[tp], hss.at[d], hrs.at[d], device)
    for device, _, source, d in x_peers:
        arrived(dn.at[source], wss.at[2, d], wrs.at[2, d], device)
    for device, _, source, d in x_peers:
        arrived(hid.at[source], hss.at[d], hrs.at[d], device)

    hidden = hid[...].reshape(ntp * ff, slots)
    down_all = dn[...].reshape(ntp * ff, share)
    h_yz = dot_nt(same, hidden).astype(BF16)
    ra[...] = dot(h_yz, down_all[:, :half]).astype(BF16).reshape(ra.shape)
    exchange(ra, ra1, yc_peers, yc, s3s.at[1], s3r.at[1])
    ra1[yc] = ra[yc]
    h_zy = dot_nt(to_zy, hidden).astype(BF16)
    rb[...] = dot(h_zy, down_all[:, half:]).astype(BF16).reshape(rb.shape)
    exchange(rb, rb1, z_peers, z, s4s.at[1], s4r.at[1])
    rb1[z] = rb[z]

    await_all(ra1, yc_peers, s3s.at[1], s3r.at[1])
    ra1p[...] = dot(to_zy, ra1[...].reshape(slots, half)).astype(BF16).reshape(ra1p.shape)
    exchange(ra1p, ra2, z_peers, z, us, ur)
    ra2[z] = ra1p[z]
    await_all(rb1, z_peers, s4s.at[1], s4r.at[1])
    rb1p[...] = dot(to_yz, rb1[...].reshape(slots, half)).astype(BF16).reshape(rb1p.shape)
    exchange(rb1p, rb2, yc_peers, yc, s3s.at[2], s3r.at[2])
    rb2[yc] = rb1p[yc]

    await_all(ra2, z_peers, us, ur)
    back = ra2[...].reshape(slots, half)
    out[:, :half] = (dot(wa_hi, back) + dot(wa_lo, back)).astype(BF16)
    await_all(rb2, yc_peers, s3s.at[2], s3r.at[2])
    back = rb2[...].reshape(slots, half)
    out[:, half:] = (dot(wb_hi, back) + dot(wb_lo, back)).astype(BF16)

    for copy in pending:
        copy.wait_send()


def body(nz, tokens, norm_gain, routes, group_prob, expert_logits, gate_weight, up_weight, down_matrix):
    tok, width = tokens.shape
    ntp = lax.axis_size("tp")
    nyc = lax.axis_size("ep") // nz
    share, half = width // ntp, width // ntp // 2
    ff = gate_weight.shape[2]
    slots = nz * nyc * CAP
    by_z = pltpu.VMEM((nz, nyc * CAP, half), BF16)
    by_yc = pltpu.VMEM((nyc, nz * CAP, half), BF16)
    vmem = pl.BlockSpec(memory_space=pltpu.VMEM)
    anywhere = pl.BlockSpec(memory_space=pl.ANY)
    dma = pltpu.SemaphoreType.DMA
    return pl.pallas_call(
        functools.partial(kernel, nz, nyc, ntp),
        out_shape=jax.ShapeDtypeStruct((tok, share), BF16),
        in_specs=[vmem] * 5 + [anywhere] * 3,
        out_specs=vmem,
        scratch_shapes=[
            pltpu.VMEM((ntp, 2 * ff, share), BF16),
            pltpu.VMEM((ntp, ff, share), BF16),
            by_z, by_yc,
            by_z, by_yc,
            by_yc, by_z,
            by_yc, by_z,
            pltpu.VMEM((ntp, 2 * ff, slots), BF16),
            pltpu.VMEM((ntp, 2 * ff, slots), BF16),
            pltpu.VMEM((ntp, ff, slots), BF16),
            by_yc, by_z,
            by_yc, by_z,
            by_z, by_yc,
            by_z, by_yc,
            dma((3,)),
            dma((3, ntp)), dma((3, ntp)),
            dma((nz,)), dma((nz,)),
            dma((nyc,)), dma((nyc,)),
            dma((ntp,)), dma((ntp,)),
            dma((ntp,)), dma((ntp,)),
            dma((3, nyc)), dma((3, nyc)),
            dma((2, nz)), dma((2, nz)),
            dma((nz,)), dma((nz,)),
        ],
        compiler_params=pltpu.CompilerParams(
            collective_id=0, has_side_effects=True, vmem_limit_bytes=40 * 2**20
        ),
    )(
        tokens,
        norm_gain.reshape(1, width),
        routes.T,
        group_prob.reshape(1, tok),
        expert_logits.T,
        jnp.swapaxes(gate_weight, 1, 2)[0],
        jnp.swapaxes(up_weight, 1, 2)[0],
        down_matrix[0],
    )


def solution(mesh, nz=8):
    return jax.shard_map(
        functools.partial(body, nz),
        mesh=mesh,
        in_specs=(
            P("ep", None),
            P(),
            P("ep", None),
            P("ep"),
            P("ep", None),
            P("ep", None, "tp"),
            P("ep", None, "tp"),
            P("ep", "tp", None),
        ),
        out_specs=P("ep", "tp"),
        check_vma=False,
    )
```

time: 137 us -> 66.6 us (0.49)
  Pallas kernels: 0 us -> 60.9 us
  waiting for transfers between devices: 57.7 us -> 0 us
  starting transfers between devices: 38.6 us -> 0 us
  local copies, waits for them, and re-layouts: 22.9 us -> 5.38 us
  other arithmetic: 15.6 us -> 0 us
  matrix products: 1.82 us -> 0 us
    pallas_call x0 -> x1, Pallas kernels: none -> 60.9 us  [body(): pl.pallas_call(functools.partial(kernel, nz, nyc, ntp), out_shape=jax.Sha...]
    all_to_all x5 -> x0, waiting for transfers between devices: 57.7 us -> none  [the longest x2 23.1 us: sent_to_all(): return lax.all_to_all(copies, axis, split_axis=0, concat_axis=0, tiled=True)]
    all_to_all x5 -> x0, starting transfers between devices: 38.6 us -> none  [the longest x1 18.4 us: body(): lax.all_to_all(my_features, 'ep', split_axis=0, concat_axis=0, tiled=True)]
    unnamed x1 -> x0, other arithmetic: 11.5 us -> none
    scatter x1 -> x0, local copies, waits for them, and re-layouts: 5.92 us -> none  [body(): jnp.zeros((experts * capacity, model_width), jnp.bfloat16).at[target]]
    reduce_sum x4 -> x0, other arithmetic: 2.8 us -> none  [the longest x1 1.36 us: body(): combined = jnp.sum(picked * weights[:, :, None], 1).astype(jnp.bfloat16)]
    reshape x2 -> x0, local copies, waits for them, and re-layouts: 2.68 us -> none  [the longest x1 2.35 us: body(): outgoing = outgoing.reshape(experts, capacity, model_width)]
    dynamic_slice x1 -> x0, local copies, waits for them, and re-layouts: 2.07 us -> none  [body(): lax.dynamic_slice_in_dim(outgoing, lax.axis_index('tp') * feature_share,...]
  transfers between devices with their start and end apart: 5 -> 0, of which waited for: 5 -> 0; matrix products, arithmetic and copies ran while one was open for 12% -> 0% of each run, Pallas kernels for 0% -> 0%
where the time goes in v1:
time: 66.6 us; the launch traced here: 66.3 us
  Pallas kernels  60.9 us (91%)
  local copies, waits for them, and re-layouts  5.38 us (8%)
    pallas_call x1, Pallas kernels, body(): pl.pallas_call(functools.partial(kernel, nz, nyc, ntp), out_shape=jax.Sha...  60.9 us
    unnamed x17, local copies, waits for them, and re-layouts  5.38 us

profile of v1, /device:TPU:1, one launch (start us, length us, event | category | flops | bytes accessed | tf_op | source)
XLA Modules:
  0.0 66.3 jit_solution(11901849077334752335)
XLA Ops:
  0.0 0.0 copy-start.4
  0.0 0.0 copy-start.6
  0.0 0.0 copy-start.5
  0.0 0.0 copy-start.7
  0.0 0.7 %copy-done.4 = f32[2048]{0:T(1024)S(1)} copy-done((f32[2048]{0:T(1024)S(1)}, f32[2048]{0:T(1024)}, u32[]{:S(2)}) %copy-start.4) | copy-done | bytes 8216
  0.7 0.0 copy-done.6
  0.7 0.0 copy-done.5
  0.7 0.0 copy-done.7
  0.7 0.0 copy-start
  0.7 1.0 %copy-done = bf16[128,2048]{1,0:T(8,128)(2,1)S(1)} copy-done((bf16[128,2048]{1,0:T(8,128)(2,1)S(1)}, bf16[128,2048]{1,0:T(8,128)(2,1)}, u32[]{:S(2)}) %copy-start) | copy-done | bytes 524312
  1.8 0.0 copy-start.1
  1.8 1.0 %copy-done.1 = bf16[1,2048,96]{1,2,0:T(8,128)(2,1)S(1)} copy-done((bf16[1,2048,96]{1,2,0:T(8,128)(2,1)S(1)}, bf16[1,2048,96]{1,2,0:T(8,128)(2,1)}, u32[]{:S(2)}) %copy-start.1) | copy-done | bytes 393240
  2.8 0.0 copy-start.2
  2.8 1.0 %copy-done.2 = bf16[1,2048,96]{1,2,0:T(8,128)(2,1)S(1)} copy-done((bf16[1,2048,96]{1,2,0:T(8,128)(2,1)S(1)}, bf16[1,2048,96]{1,2,0:T(8,128)(2,1)}, u32[]{:S(2)}) %copy-start.2) | copy-done | bytes 393240
  3.7 0.0 copy-start.3
  3.8 1.0 %copy-done.3 = bf16[1,96,2048]{2,1,0:T(8,128)(2,1)S(1)} copy-done((bf16[1,96,2048]{2,1,0:T(8,128)(2,1)S(1)}, bf16[1,96,2048]{2,1,0:T(8,128)(2,1)}, u32[]{:S(2)}) %copy-start.3) | copy-done | bytes 393240
  4.7 60.9 %shard_map.82 = bf16[128,512]{1,0:T(8,128)(2,1)S(1)} custom-call(bf16[128,2048]{1,0:T(8,128)(2,1)S(1)} %copy-done, f32[1,2048]{1,0:T(1,128)S(1)} %bitcast.14, s32[2,128]{1,0:T(2,128)S(1)} %bitcast.15, f32[1,128]{1,0:T(1,128)S(1)} %bitcast.17, f32[2,128]{1,0:T(2,128)S(1)} %bitcast.16, bf16[96,2048]{1,0:T(8,128)(2,1)S(1)} %bitcast.11, ...), custom_call_target="tpu_custom_call" | custom-call | tf_op jit(solution)/shard_map/pallas_call | solution.py:251
  65.6 0.7 copy.10
Async XLA Ops:
  0.0 0.7 %copy-start.4 = (f32[2048]{0:T(1024)S(1)}, f32[2048]{0:T(1024)}, u32[]{:S(2)}) copy-start(f32[2048]{0:T(1024)} %param.9) | copy-start | bytes 24580
  0.0 0.7 %copy-start.6 = (f32[128,2]{0,1:T(2,128)S(1)}, f32[128,2]{0,1:T(2,128)}, u32[]{:S(2)}) copy-start(f32[128,2]{0,1:T(2,128)} %param.12) | copy-start | bytes 3076
  0.0 0.7 %copy-start.5 = (s32[128,2]{0,1:T(2,128)S(1)}, s32[128,2]{0,1:T(2,128)}, u32[]{:S(2)}) copy-start(s32[128,2]{0,1:T(2,128)} %param.10) | copy-start | bytes 3076
  0.0 0.7 %copy-start.7 = (f32[128]{0:T(128)S(1)}, f32[128]{0:T(128)}, u32[]{:S(2)}) copy-start(f32[128]{0:T(128)} %param.11) | copy-start | bytes 1540
  0.7 1.0 %copy-start = (bf16[128,2048]{1,0:T(8,128)(2,1)S(1)}, bf16[128,2048]{1,0:T(8,128)(2,1)}, u32[]{:S(2)}) copy-start(bf16[128,2048]{1,0:T(8,128)(2,1)} %tokens.1) | copy-start | bytes 1572868
  1.8 1.0 %copy-start.1 = (bf16[1,2048,96]{1,2,0:T(8,128)(2,1)S(1)}, bf16[1,2048,96]{1,2,0:T(8,128)(2,1)}, u32[]{:S(2)}) copy-start(bf16[1,2048,96]{1,2,0:T(8,128)(2,1)} %param.13) | copy-start | bytes 1179652
  2.8 1.0 %copy-start.2 = (bf16[1,2048,96]{1,2,0:T(8,128)(2,1)S(1)}, bf16[1,2048,96]{1,2,0:T(8,128)(2,1)}, u32[]{:S(2)}) copy-start(bf16[1,2048,96]{1,2,0:T(8,128)(2,1)} %param.14) | copy-start | bytes 1179652
  3.7 1.0 %copy-start.3 = (bf16[1,96,2048]{2,1,0:T(8,128)(2,1)S(1)}, bf16[1,96,2048]{2,1,0:T(8,128)(2,1)}, u32[]{:S(2)}) copy-start(bf16[1,96,2048]{2,1,0:T(8,128)(2,1)} %param.15) | copy-start | bytes 1179652

commit v2 on v1

v2 whole, which is shorter than its diff:
```python
import functools

import jax
import jax.numpy as jnp
from jax import lax
from jax.experimental import pallas as pl
from jax.experimental.pallas import tpu as pltpu
from jax.sharding import PartitionSpec as P

MESH = pl.DeviceIdType.MESH
CAP = 3
CORES = 2
F32, BF16 = jnp.float32, jnp.bfloat16
A1, B1, A2, B2, C1, D1, C2, D2, PS, HI, WG = range(0, 11 * CAP, CAP)
DN = WG + 1


def quotient(values, divisor):
    return lax.shift_right_logical(values * ((65535 + divisor) // divisor), 16)


def far_first(n):
    return sorted(range(1, n), key=lambda d: -min(d, n - d))


def dot(a, b):
    return jnp.dot(a, b, preferred_element_type=F32)


def dot_nt(a, b):
    return lax.dot_general(a, b, (((1,), (1,)), ((), ())), preferred_element_type=F32)


def kernel(
    nz, nyc, ntp,
    tokens_hbm, gain_hbm, routes_hbm, prob_hbm, logits_hbm, gate, up, down,
    out,
    tokens, gain, routes, prob, logits,
    wg, dn, oa, ob, a1, b1, a1p, b1p, a2, b2, ps, pr, hid, ra, rb, ra1, rb1, ra1p, rb1p, ra2, rb2,
    lsem, ssem, rsem,
):
    ny = nyc // CORES
    ep, tp = lax.axis_index("ep"), lax.axis_index("tp")
    z, yc = lax.div(ep, nyc), lax.rem(ep, nyc)
    y, core = lax.div(yc, CORES), lax.rem(yc, CORES)
    tok, width = tokens_hbm.shape
    share = width // ntp
    half = share // 2
    ff = gate.shape[0]
    experts = nz * nyc

    z_steps = far_first(nz)
    yc_steps = [(dy, dc) for dy in [*far_first(ny), 0] for dc in range(CORES) if dy or dc]
    x_steps = far_first(ntp)

    def z_to(d):
        return lax.rem(z + d, nz)

    def yc_to(dy, dc):
        return lax.rem(y + dy, ny) * CORES + lax.rem(core + dc, CORES)

    def x_to(d):
        return lax.rem(tp + d, ntp)

    z_peers = [((z_to(d) * nyc + yc, tp), z_to(d), d) for d in z_steps]
    yc_peers = [((z * nyc + yc_to(*d), tp), yc_to(*d), d) for d in yc_steps]
    x_peers = [((ep, x_to(d)), x_to(d), d) for d in x_steps]
    others = pl.ds(1, ntp - 1)

    def columns(j):
        return pl.ds(pl.multiple_of(j * share, share), share)

    inputs = [
        pltpu.make_async_copy(routes_hbm, routes, lsem.at[0]),
        pltpu.make_async_copy(tokens_hbm, tokens, lsem.at[1]),
        pltpu.make_async_copy(gain_hbm.at[:, columns(tp)], gain, lsem.at[2]),
        pltpu.make_async_copy(prob_hbm, prob, lsem.at[3]),
        pltpu.make_async_copy(logits_hbm, logits, lsem.at[4]),
    ]
    for copy in inputs:
        copy.start()

    barrier = pltpu.get_barrier_semaphore()
    for device, *_ in [*z_peers, *yc_peers, *x_peers]:
        pl.semaphore_signal(barrier, inc=1, device_id=device, device_id_type=MESH)

    pending = []

    def remote(src, dst, sems, device):
        return pltpu.make_async_remote_copy(
            src_ref=src, dst_ref=dst, send_sem=sems[0], recv_sem=sems[1], device_id=device, device_id_type=MESH
        )

    def send(src, dst, sems, device):
        remote(src, dst, sems, device).start()

    def pair(number):
        return ssem.at[number], rsem.at[number]

    def exchange(c, src, dst, peers, mine, number):
        sems = pair(number + c)
        for device, there, _ in peers:
            send(src.at[c, there], dst.at[c, mine], sems, device)
        dst[c, mine] = src[c, mine]
        pending.append(remote(src.at[c, pl.ds(0, len(peers))], src.at[c, pl.ds(0, len(peers))], sems, device))

    def await_all(c, dst, peers, number):
        everything = dst.at[c, pl.ds(0, len(peers))]
        remote(everything, everything, pair(number + c), peers[0][0]).wait_recv()

    local = [
        pltpu.make_async_copy(gate.at[:, columns(tp)], wg.at[0, pl.ds(0, ff)], lsem.at[5]),
        pltpu.make_async_copy(up.at[:, columns(tp)], wg.at[0, pl.ds(ff, ff)], lsem.at[6]),
        pltpu.make_async_copy(down.at[:, columns(tp)], dn.at[0], lsem.at[7]),
    ]
    for copy in local:
        copy.start()

    inputs[0].wait()
    r0, r1 = routes[0:1, :], routes[1:2, :]
    ids = lax.broadcasted_iota(jnp.int32, (experts, tok), 0)
    is0, is1 = ids == r0, ids == r1
    e0, e1 = is0.astype(F32), is1.astype(F32)
    before = (
        lax.broadcasted_iota(jnp.int32, (tok, tok), 0) < lax.broadcasted_iota(jnp.int32, (tok, tok), 1)
    ).astype(BF16)
    earlier = dot((e0 + e1).astype(BF16), before)
    c0 = jnp.sum(earlier * e0, 0, keepdims=True)
    c1 = jnp.sum(earlier * e1, 0, keepdims=True)

    def turned(r):
        rz = quotient(r, nyc)
        return (r - rz * nyc) * nz + rz

    is0b, is1b = ids == turned(r0), ids == turned(r1)

    inputs[1].wait()
    inputs[2].wait()
    values = tokens[...].astype(F32)
    scale = lax.rsqrt(jnp.sum(values * values, -1, keepdims=True) * (1.0 / width) + 1e-06)
    normed = (tokens[:, columns(tp)].astype(F32) * scale * gain[...]).astype(BF16)

    for c in range(CAP):
        in0, in1 = c0 == c, c1 == c
        pick = ((is0 & in0) | (is1 & in1)).astype(BF16)
        oa[c] = dot(pick, normed[:, :half]).astype(BF16).reshape(oa.shape[1:])
        pick = ((is0b & in0) | (is1b & in1)).astype(BF16)
        ob[c] = dot(pick, normed[:, half:]).astype(BF16).reshape(ob.shape[1:])

    pl.semaphore_wait(barrier, len(z_peers) + len(yc_peers) + len(x_peers))

    for c in range(CAP):
        exchange(c, oa, a1, z_peers, z, A1)
        exchange(c, ob, b1, yc_peers, yc, B1)
        if c == 0:
            for device, there, d in x_peers:
                send(gate.at[:, columns(there)], wg.at[d, pl.ds(0, ff)], pair(WG), device)
                send(up.at[:, columns(there)], wg.at[d, pl.ds(ff, ff)], pair(WG), device)
            gates_and_ups = remote(wg.at[others], wg.at[others], pair(WG), device)
    for device, there, d in x_peers:
        send(down.at[:, columns(there)], dn.at[d], pair(DN), device)
    downs = remote(dn.at[others], dn.at[others], pair(DN), device)
    pending += [gates_and_ups, downs]

    to = lax.broadcasted_iota(jnp.int32, (experts, experts), 0)
    of = lax.broadcasted_iota(jnp.int32, (experts, experts), 1)

    def reorder(outer, inner):
        i = quotient(to, inner)
        return (of == (to - i * inner) * outer + i).astype(BF16)

    to_yz, to_zy = reorder(nyc, nz), reorder(nz, nyc)
    same = (of == to).astype(BF16)

    def reordered(c, matrix, src, dst):
        dst[c] = dot(matrix, src[c].reshape(experts, half)).astype(BF16).reshape(dst.shape[1:])

    for c in range(CAP):
        await_all(c, a1, z_peers, A1)
        reordered(c, to_yz, a1, a1p)
        exchange(c, a1p, a2, yc_peers, yc, A2)
        await_all(c, b1, yc_peers, B1)
        reordered(c, to_zy, b1, b1p)
        exchange(c, b1p, b2, z_peers, z, B2)

    inputs[3].wait()
    inputs[4].wait()
    top = jnp.maximum(logits[0:1, :], logits[1:2, :])
    x0, x1 = jnp.exp(logits[0:1, :] - top), jnp.exp(logits[1:2, :] - top)
    w0, w1 = prob[...] * (x0 / (x0 + x1)), prob[...] * (x1 / (x0 + x1))
    zero = jnp.zeros((experts, tok), F32)

    def split(at0, at1):
        whole = (jnp.where(at0, w0, zero) + jnp.where(at1, w1, zero)).T
        high = whole.astype(BF16)
        return high, (whole - high.astype(F32)).astype(BF16)

    mix_a = [split(is0 & (c0 == c), is1 & (c1 == c)) for c in range(CAP)]
    mix_b = [split(is0b & (c0 == c), is1b & (c1 == c)) for c in range(CAP)]

    for copy in local:
        copy.wait()
    gates_and_ups.wait_recv()

    own = []
    for c in range(CAP):
        await_all(c, a2, yc_peers, A2)
        await_all(c, b2, z_peers, B2)
        xa = a2[c].reshape(experts, half)
        xb = dot(to_yz, b2[c].reshape(experts, half)).astype(BF16)

        def partial(d):
            return dot_nt(wg[d, :, :half], xa) + dot_nt(wg[d, :, half:], xb)

        for device, _, d in x_peers:
            ps[c, d] = partial(ntp - d).astype(BF16)
            send(ps.at[c, d], pr.at[c, d], pair(PS + c), device)
        pending.append(remote(ps.at[c, others], pr.at[c, others], pair(PS + c), device))
        own.append((partial(0), pending[-1]))

    blocks = []
    for c in range(CAP):
        total, parts = own[c]
        parts.wait_recv()
        for d in range(1, ntp):
            total = total + pr[c, d].astype(F32)
        g, u = total[:ff], total[ff:]
        hid[c, 0] = (g / (1.0 + jnp.exp(-g)) * u).astype(BF16)
        for device, _, d in x_peers:
            send(hid.at[c, 0], hid.at[c, d], pair(HI + c), device)
        blocks.append(remote(hid.at[c, others], hid.at[c, others], pair(HI + c), device))
    pending += blocks

    downs.wait_recv()
    down_all = dn[...].reshape(ntp * ff, share)

    for c in range(CAP):
        blocks[c].wait_recv()
        hidden = hid[c].reshape(ntp * ff, experts)
        h_yz = dot_nt(same, hidden).astype(BF16)
        ra[c] = dot(h_yz, down_all[:, :half]).astype(BF16).reshape(ra.shape[1:])
        exchange(c, ra, ra1, yc_peers, yc, C1)
        h_zy = dot_nt(to_zy, hidden).astype(BF16)
        rb[c] = dot(h_zy, down_all[:, half:]).astype(BF16).reshape(rb.shape[1:])
        exchange(c, rb, rb1, z_peers, z, D1)

    for c in range(CAP):
        await_all(c, ra1, yc_peers, C1)
        reordered(c, to_zy, ra1, ra1p)
        exchange(c, ra1p, ra2, z_peers, z, C2)
        await_all(c, rb1, z_peers, D1)
        reordered(c, to_yz, rb1, rb1p)
        exchange(c, rb1p, rb2, yc_peers, yc, D2)

    sum_a, sum_b = 0.0, 0.0
    for c in range(CAP):
        await_all(c, ra2, z_peers, C2)
        back = ra2[c].reshape(experts, half)
        sum_a = sum_a + (dot(mix_a[c][0], back) + dot(mix_a[c][1], back))
        await_all(c, rb2, yc_peers, D2)
        back = rb2[c].reshape(experts, half)
        sum_b = sum_b + (dot(mix_b[c][0], back) + dot(mix_b[c][1], back))
    out[:, :half] = sum_a.astype(BF16)
    out[:, half:] = sum_b.astype(BF16)

    for copy in pending:
        copy.wait_send()


def body(nz, tokens, norm_gain, routes, group_prob, expert_logits, gate_weight, up_weight, down_matrix):
    tok, width = tokens.shape
    ntp = lax.axis_size("tp")
    nyc = lax.axis_size("ep") // nz
    share, half = width // ntp, width // ntp // 2
    ff = gate_weight.shape[2]
    experts = nz * nyc
    by_z = pltpu.VMEM((CAP, nz, nyc, half), BF16)
    by_yc = pltpu.VMEM((CAP, nyc, nz, half), BF16)
    dma = pltpu.SemaphoreType.DMA
    return pl.pallas_call(
        functools.partial(kernel, nz, nyc, ntp),
        out_shape=jax.ShapeDtypeStruct((tok, share), BF16),
        in_specs=[pl.BlockSpec(memory_space=pltpu.HBM)] * 8,
        out_specs=pl.BlockSpec(memory_space=pltpu.VMEM),
        scratch_shapes=[
            pltpu.VMEM((tok, width), BF16),
            pltpu.VMEM((1, share), F32),
            pltpu.VMEM((2, tok), jnp.int32),
            pltpu.VMEM((1, tok), F32),
            pltpu.VMEM((2, tok), F32),
            pltpu.VMEM((ntp, 2 * ff, share), BF16),
            pltpu.VMEM((ntp, ff, share), BF16),
            by_z, by_yc,
            by_z, by_yc,
            by_yc, by_z,
            by_yc, by_z,
            pltpu.VMEM((CAP, ntp, 2 * ff, experts), BF16),
            pltpu.VMEM((CAP, ntp, 2 * ff, experts), BF16),
            pltpu.VMEM((CAP, ntp, ff, experts), BF16),
            by_yc, by_z,
            by_yc, by_z,
            by_z, by_yc,
            by_z, by_yc,
            dma((8,)),
            dma((DN + 1,)), dma((DN + 1,)),
        ],
        compiler_params=pltpu.CompilerParams(
            collective_id=0, has_side_effects=True, vmem_limit_bytes=67043328
        ),
    )(
        tokens,
        norm_gain.reshape(1, width),
        routes.T,
        group_prob.reshape(1, tok),
        expert_logits.T,
        jnp.swapaxes(gate_weight, 1, 2)[0],
        jnp.swapaxes(up_weight, 1, 2)[0],
        down_matrix[0],
    )


def solution(mesh, nz=8):
    return jax.shard_map(
        functools.partial(body, nz),
        mesh=mesh,
        in_specs=(
            P("ep", None),
            P(),
            P("ep", None),
            P("ep"),
            P("ep", None),
            P("ep", None, "tp"),
            P("ep", None, "tp"),
            P("ep", "tp", None),
        ),
        out_specs=P("ep", "tp"),
        check_vma=False,
    )
```

time: 66.6 us -> 54.5 us (0.82)
  Pallas kernels: 60.9 us -> 52.8 us
  local copies, waits for them, and re-layouts: 5.38 us -> 1.57 us
    pallas_call x1, Pallas kernels: 60.9 us -> 52.8 us  [body(): pl.pallas_call(functools.partial(kernel, nz, nyc, ntp), out_shape=jax.Sha...]
    unnamed x17 -> x1, local copies, waits for them, and re-layouts: 5.38 us -> 1.57 us
where the time goes in v2:
time: 54.5 us; the launch traced here: 54.4 us
  Pallas kernels  52.8 us (97%)
  local copies, waits for them, and re-layouts  1.57 us (3%)
    pallas_call x1, Pallas kernels, body(): pl.pallas_call(functools.partial(kernel, nz, nyc, ntp), out_shape=jax.Sha...  52.8 us
    unnamed x1, local copies, waits for them, and re-layouts  1.57 us

profile of v2, /device:TPU:1, one launch (start us, length us, event | category | flops | bytes accessed | tf_op | source)
XLA Modules:
  0.0 54.4 jit_solution(4464890598616085736)
XLA Ops:
  0.0 52.8 %shard_map.82 = bf16[128,512]{1,0:T(8,128)(2,1)} custom-call(bf16[128,2048]{1,0:T(8,128)(2,1)} %tokens_hbm.1, f32[1,2048]{1,0:T(1,128)} %bitcast.14, s32[2,128]{1,0:T(2,128)} %bitcast.15, f32[1,128]{1,0:T(1,128)} %bitcast.17, f32[2,128]{1,0:T(2,128)} %bitcast.16, bf16[96,2048]{1,0:T(8,128)(2,1)} %bitcast.11, bf16[96,2048]{1,0:T(8,128)(2,1)} %bitcast.12, ...), custom_call_target="tpu_custom_call" | custom-call | tf_op jit(solution)/shard_map/pallas_call | solution.py:280
  52.8 1.6 %copy.10 = bf16[128,512]{1,0:T(8,128)(2,1)} copy(bf16[128,512]{1,0:T(8,128)(2,1)} %shard_map.82) | data formatting | bytes 262144

commit v3 on v2

--- a/solution.py
+++ b/solution.py
@@ -13,6 +13,7 @@
 F32, BF16 = jnp.float32, jnp.bfloat16
 A1, B1, A2, B2, C1, D1, C2, D2, PS, HI, WG = range(0, 11 * CAP, CAP)
 DN = WG + 1
+CHUNKS = ((0, 0), (0, 1)), ((1, 0), (2, 0)), ((1, 1), (2, 1))
 
 
 def quotient(values, divisor):
@@ -48,6 +49,7 @@
     half = share // 2
     ff = gate.shape[0]
     experts = nz * nyc
+    side, rows = nz // 2, experts // 2
 
     z_steps = far_first(nz)
     yc_steps = [(dy, dc) for dy in [*far_first(ny), 0] for dc in range(CORES) if dy or dc]
@@ -202,55 +204,92 @@
         copy.wait()
     gates_and_ups.wait_recv()
 
-    own = []
-    for c in range(CAP):
-        await_all(c, a2, yc_peers, A2)
-        await_all(c, b2, z_peers, B2)
-        xa = a2[c].reshape(experts, half)
-        xb = dot(to_yz, b2[c].reshape(experts, half)).astype(BF16)
+    own, here = [], set()
+    for k, blocks in enumerate(CHUNKS):
+        for c in sorted({c for c, _ in blocks} - here):
+            await_all(c, a2, yc_peers, A2)
+            await_all(c, b2, z_peers, B2)
+            here.add(c)
+        xa = [
+            dot(to_zy[h * rows : (h + 1) * rows], a2[c].reshape(experts, half)).astype(BF16) for c, h in blocks
+        ]
+        xb = [b2[c, pl.ds(h * side, side)].reshape(rows, half) for c, h in blocks]
+        xa, xb = jnp.concatenate(xa, 0), jnp.concatenate(xb, 0)
 
         def partial(d):
             return dot_nt(wg[d, :, :half], xa) + dot_nt(wg[d, :, half:], xb)
 
         for device, _, d in x_peers:
-            ps[c, d] = partial(ntp - d).astype(BF16)
-            send(ps.at[c, d], pr.at[c, d], pair(PS + c), device)
-        pending.append(remote(ps.at[c, others], pr.at[c, others], pair(PS + c), device))
+            ps[k, d] = partial(ntp - d).astype(BF16)
+            send(ps.at[k, d], pr.at[k, d], pair(PS + k), device)
+        pending.append(remote(ps.at[k, others], pr.at[k, others], pair(PS + k), device))
         own.append((partial(0), pending[-1]))
 
-    blocks = []
-    for c in range(CAP):
-        total, parts = own[c]
+    gathered = []
+    for k in range(CAP):
+        total, parts = own[k]
         parts.wait_recv()
         for d in range(1, ntp):
-            total = total + pr[c, d].astype(F32)
+            total = total + pr[k, d].astype(F32)
         g, u = total[:ff], total[ff:]
-        hid[c, 0] = (g / (1.0 + jnp.exp(-g)) * u).astype(BF16)
+        hid[k, 0] = (g / (1.0 + jnp.exp(-g)) * u).astype(BF16)
         for device, _, d in x_peers:
-            send(hid.at[c, 0], hid.at[c, d], pair(HI + c), device)
-        blocks.append(remote(hid.at[c, others], hid.at[c, others], pair(HI + c), device))
-    pending += blocks
+            send(hid.at[k, 0], hid.at[k, d], pair(HI + k), device)
+        gathered.append(remote(hid.at[k, others], hid.at[k, others], pair(HI + k), device))
+    pending += gathered
+
+    def to_halves(k, src, dst, number):
+        for b, (c, h) in enumerate(CHUNKS[k]):
+            for j in range(side):
+                there = h * side + j
+
+                @pl.when(z != there)
+                def _(b=b, c=c, j=j, there=there):
+                    send(src.at[k, b * side + j], dst.at[c, z], pair(number + c), (there * nyc + yc, tp))
+
+                @pl.when(z == there)
+                def _(b=b, c=c, j=j, there=there):
+                    dst[c, there] = src[k, b * side + j]
 
     downs.wait_recv()
     down_all = dn[...].reshape(ntp * ff, share)
 
-    for c in range(CAP):
-        blocks[c].wait_recv()
-        hidden = hid[c].reshape(ntp * ff, experts)
-        h_yz = dot_nt(same, hidden).astype(BF16)
-        ra[c] = dot(h_yz, down_all[:, :half]).astype(BF16).reshape(ra.shape[1:])
-        exchange(c, ra, ra1, yc_peers, yc, C1)
-        h_zy = dot_nt(to_zy, hidden).astype(BF16)
-        rb[c] = dot(h_zy, down_all[:, half:]).astype(BF16).reshape(rb.shape[1:])
-        exchange(c, rb, rb1, z_peers, z, D1)
-
-    for c in range(CAP):
-        await_all(c, ra1, yc_peers, C1)
-        reordered(c, to_zy, ra1, ra1p)
-        exchange(c, ra1p, ra2, z_peers, z, C2)
-        await_all(c, rb1, z_peers, D1)
-        reordered(c, to_yz, rb1, rb1p)
-        exchange(c, rb1p, rb2, yc_peers, yc, D2)
+    for k in range(CAP):
+        gathered[k].wait_recv()
+        hidden = hid[k].reshape(ntp * ff, experts)
+        h_yz = dot_nt(to_yz, hidden).astype(BF16)
+        ra[k] = dot(h_yz, down_all[:, :half]).astype(BF16).reshape(ra.shape[1:])
+        exchange(k, ra, ra1, yc_peers, yc, C1)
+        h_zy = dot_nt(same, hidden).astype(BF16)
+        rb[k] = dot(h_zy, down_all[:, half:]).astype(BF16).reshape(rb.shape[1:])
+        to_halves(k, rb, rb1, D1)
+
+    def forward_a(k):
+        await_all(k, ra1, yc_peers, C1)
+        reordered(k, to_zy, ra1, ra1p)
+        to_halves(k, ra1p, ra2, C2)
+
+    def forward_b(*slots):
+        for c in slots:
+            await_all(c, rb1, z_peers, D1)
+            reordered(c, to_yz, rb1, rb1p)
+            for device, there, _ in yc_peers:
+                send(rb1p.at[c, there], rb2.at[c, yc], pair(D2 + c), device)
+            rb2[c, yc] = rb1p[c, yc]
+
+    def in_half(h):
+        return lax.div(z, side) == h
+
+    for k, blocks in enumerate(CHUNKS):
+        forward_a(k)
+        for h in range(2):
+            slots = [c for c, of_half in blocks if of_half == h]
+            if slots:
+                pl.when(in_half(h))(functools.partial(forward_b, *slots))
+    for c in range(CAP):
+        for src, peers, number in ((rb, z_peers, D1), (ra1p, z_peers, C2), (rb1p, yc_peers, D2)):
+            everything = src.at[c, pl.ds(0, len(peers))]
+            pending.append(remote(everything, everything, pair(number + c), peers[0][0]))
 
     sum_a, sum_b = 0.0, 0.0
     for c in range(CAP):
@@ -305,17 +344,17 @@
             dma((DN + 1,)), dma((DN + 1,)),
         ],
         compiler_params=pltpu.CompilerParams(
-            collective_id=0, has_side_effects=True, vmem_limit_bytes=67043328
+            collective_id=0, has_side_effects=True, vmem_limit_bytes=40 * 2**20
         ),
     )(
-        tokens,
-        norm_gain.reshape(1, width),
-        routes.T,
-        group_prob.reshape(1, tok),
-        expert_logits.T,
-        jnp.swapaxes(gate_weight, 1, 2)[0],
-        jnp.swapaxes(up_weight, 1, 2)[0],
-        down_matrix[0],
+        pltpu.with_memory_space_constraint(tokens, pltpu.HBM),
+        pltpu.with_memory_space_constraint(norm_gain.reshape(1, width), pltpu.HBM),
+        pltpu.with_memory_space_constraint(routes.T, pltpu.HBM),
+        pltpu.with_memory_space_constraint(group_prob.reshape(1, tok), pltpu.HBM),
+        pltpu.with_memory_space_constraint(expert_logits.T, pltpu.HBM),
+        pltpu.with_memory_space_constraint(jnp.swapaxes(gate_weight, 1, 2)[0], pltpu.HBM),
+        pltpu.with_memory_space_constraint(jnp.swapaxes(up_weight, 1, 2)[0], pltpu.HBM),
+        pltpu.with_memory_space_constraint(down_matrix[0], pltpu.HBM),
     )
 
 

time: 54.5 us -> 52 us (0.954)
  Pallas kernels: 52.8 us -> 51.2 us
  local copies, waits for them, and re-layouts: 1.57 us -> 0.66 us
    pallas_call x1, Pallas kernels: 52.8 us -> 51.2 us  [body(): pl.pallas_call(functools.partial(kernel, nz, nyc, ntp), out_shape=jax.Sha...]
    unnamed x1, local copies, waits for them, and re-layouts: 1.57 us -> 0.66 us
where the time goes in v3:
time: 52 us; the launch traced here: 51.8 us
  Pallas kernels  51.2 us (98%)
  local copies, waits for them, and re-layouts  0.66 us (1%)
    pallas_call x1, Pallas kernels, body(): pl.pallas_call(functools.partial(kernel, nz, nyc, ntp), out_shape=jax.Sha...  51.2 us

profile of v3, /device:TPU:1, one launch (start us, length us, event | category | flops | bytes accessed | tf_op | source)
XLA Modules:
  0.0 51.8 jit_solution(10565210741351373491)
XLA Ops:
  0.0 51.2 %shard_map.82 = bf16[128,512]{1,0:T(8,128)(2,1)S(1)} custom-call(bf16[128,2048]{1,0:T(8,128)(2,1)} %tokens_hbm.1, f32[1,2048]{1,0:T(1,128)} %bitcast.14, s32[2,128]{1,0:T(2,128)} %bitcast.15, f32[1,128]{1,0:T(1,128)} %bitcast.17, f32[2,128]{1,0:T(2,128)} %bitcast.16, bf16[96,2048]{1,0:T(8,128)(2,1)} %bitcast.11, bf16[96,2048]{1,0:T(8,128)(2,1)} %bitcast.12, ...), custom_call_target="tpu_custom_call" | custom-call | tf_op jit(solution)/shard_map/pallas_call | solution.py:319
  51.2 0.7 %copy.10 = bf16[128,512]{1,0:T(8,128)(2,1)} copy(bf16[128,512]{1,0:T(8,128)(2,1)S(1)} %shard_map.82) | data formatting | bytes 262144

commit v4 on v3

--- a/solution.py
+++ b/solution.py
@@ -11,9 +11,25 @@
 CAP = 3
 CORES = 2
 F32, BF16 = jnp.float32, jnp.bfloat16
-A1, B1, A2, B2, C1, D1, C2, D2, PS, HI, WG = range(0, 11 * CAP, CAP)
+A1, B1, A2, B2, RE = range(0, 5 * CAP, CAP)
+CHUNKS = ((0, 0), (0, 1)), ((1, 0), (2, 0)), ((1, 1),), ((2, 1),)
+NK = len(CHUNKS)
+ORDER = [
+    ("start", 0),
+    ("start", 1),
+    ("start", 2),
+    ("finish", 0),
+    ("finish", 1),
+    ("start", 3),
+    ("finish", 2),
+    ("down", 0),
+    ("down", 1),
+    ("finish", 3),
+    ("down", 2),
+    ("down", 3),
+]
+PS, HI, WG = range(5 * CAP, 5 * CAP + 3 * NK, NK)
 DN = WG + 1
-CHUNKS = ((0, 0), (0, 1)), ((1, 0), (2, 0)), ((1, 1), (2, 1))
 
 
 def quotient(values, divisor):
@@ -37,7 +53,7 @@
     tokens_hbm, gain_hbm, routes_hbm, prob_hbm, logits_hbm, gate, up, down,
     out,
     tokens, gain, routes, prob, logits,
-    wg, dn, oa, ob, a1, b1, a1p, b1p, a2, b2, ps, pr, hid, ra, rb, ra1, rb1, ra1p, rb1p, ra2, rb2,
+    wg, dn, oa, ob, a1, b1, a1p, b1p, a2, b2, ps, pr, hid, leaving, back,
     lsem, ssem, rsem,
 ):
     ny = nyc // CORES
@@ -197,15 +213,26 @@
         high = whole.astype(BF16)
         return high, (whole - high.astype(F32)).astype(BF16)
 
-    mix_a = [split(is0 & (c0 == c), is1 & (c1 == c)) for c in range(CAP)]
-    mix_b = [split(is0b & (c0 == c), is1b & (c1 == c)) for c in range(CAP)]
+    column = lax.broadcasted_iota(jnp.int32, (experts, 2 * experts), 1)
+    expert = lax.broadcasted_iota(jnp.int32, (experts, 2 * experts), 0)
+    spread = [(column == 2 * expert + h).astype(BF16) for h in range(2)]
+    row = lax.broadcasted_iota(jnp.int32, (2 * experts, experts), 0)
+    source = lax.broadcasted_iota(jnp.int32, (2 * experts, experts), 1)
+    woven = [(row == 2 * source + h).astype(BF16) for h in range(2)]
+    mix = [
+        [[dot(part, spread[h]).astype(BF16) for part in split(is0 & (c0 == c), is1 & (c1 == c))] for h in range(2)]
+        for c in range(CAP)
+    ]
 
     for copy in local:
         copy.wait()
     gates_and_ups.wait_recv()
 
-    own, here = [], set()
-    for k, blocks in enumerate(CHUNKS):
+    own, gathered, here = {}, {}, set()
+    low = lax.broadcasted_iota(jnp.int32, (ff, experts), 1) < rows
+
+    def start_partials(k):
+        blocks = CHUNKS[k]
         for c in sorted({c for c, _ in blocks} - here):
             await_all(c, a2, yc_peers, A2)
             await_all(c, b2, z_peers, B2)
@@ -214,93 +241,90 @@
             dot(to_zy[h * rows : (h + 1) * rows], a2[c].reshape(experts, half)).astype(BF16) for c, h in blocks
         ]
         xb = [b2[c, pl.ds(h * side, side)].reshape(rows, half) for c, h in blocks]
-        xa, xb = jnp.concatenate(xa, 0), jnp.concatenate(xb, 0)
+        single = len(blocks) == 1
+        xa, xb = jnp.concatenate(xa * (1 + single), 0), jnp.concatenate(xb * (1 + single), 0)
 
         def partial(d):
-            return dot_nt(wg[d, :, :half], xa) + dot_nt(wg[d, :, half:], xb)
-
+            both = dot_nt(wg[d, :, :half], xa) + dot_nt(wg[d, :, half:], xb)
+            return jnp.where(low, both[:ff], both[ff:]) if single else both
+
+        used = pl.ds(0, ff if single else 2 * ff)
         for device, _, d in x_peers:
-            ps[k, d] = partial(ntp - d).astype(BF16)
-            send(ps.at[k, d], pr.at[k, d], pair(PS + k), device)
-        pending.append(remote(ps.at[k, others], pr.at[k, others], pair(PS + k), device))
-        own.append((partial(0), pending[-1]))
-
-    gathered = []
-    for k in range(CAP):
+            ps[k, d, used] = partial(ntp - d).astype(BF16)
+            send(ps.at[k, d, used], pr.at[k, d, used], pair(PS + k), device)
+        pending.append(remote(ps.at[k, others, used], pr.at[k, others, used], pair(PS + k), device))
+        own[k] = partial(0), pending[-1]
+
+    def finish_partials(k):
+        single = len(CHUNKS[k]) == 1
         total, parts = own[k]
         parts.wait_recv()
         for d in range(1, ntp):
-            total = total + pr[k, d].astype(F32)
-        g, u = total[:ff], total[ff:]
-        hid[k, 0] = (g / (1.0 + jnp.exp(-g)) * u).astype(BF16)
+            total = total + pr[k, d, pl.ds(0, ff if single else 2 * ff)].astype(F32)
+        if single:
+            other = jnp.roll(total, rows, 1)
+            g, u = jnp.where(low, total, other), jnp.where(low, other, total)
+        else:
+            g, u = total[:ff], total[ff:]
+        h = g / (1.0 + jnp.exp(-g)) * u
+        if single:
+            h = jnp.where(low[: ff // 2], h[: ff // 2], h[ff // 2 :])
+        used = pl.ds(0, h.shape[0])
+        hid[k, 0, used] = h.astype(BF16)
         for device, _, d in x_peers:
-            send(hid.at[k, 0], hid.at[k, d], pair(HI + k), device)
-        gathered.append(remote(hid.at[k, others], hid.at[k, others], pair(HI + k), device))
-    pending += gathered
-
-    def to_halves(k, src, dst, number):
+            send(hid.at[k, 0, used], hid.at[k, d, used], pair(HI + k), device)
+        gathered[k] = remote(hid.at[k, others, used], hid.at[k, others, used], pair(HI + k), device)
+        pending.append(gathered[k])
+
+    def apply_down(k):
+        gathered[k].wait_recv()
+        if len(CHUNKS[k]) == 1:
+            hidden = dot_nt(same, hid[k, :, pl.ds(0, ff // 2)].reshape(ntp * ff // 2, experts)).astype(BF16)
+            first = dn[:, pl.ds(0, ff // 2)].reshape(ntp * ff // 2, share)
+            second = dn[:, pl.ds(ff // 2, ff // 2)].reshape(ntp * ff // 2, share)
+            result = (dot(hidden[:rows], first) + dot(hidden[rows:], second)).astype(BF16)
+        else:
+            hidden = dot_nt(same, hid[k].reshape(ntp * ff, experts)).astype(BF16)
+            result = dot(hidden, dn[...].reshape(ntp * ff, share)).astype(BF16)
+        n = result.shape[0]
+        leaving[k, pl.ds(0, n)] = (
+            (dot(woven[0][: 2 * n, :n], result[:, :half]) + dot(woven[1][: 2 * n, :n], result[:, half:]))
+            .astype(BF16)
+            .reshape(n, 2, half)
+        )
         for b, (c, h) in enumerate(CHUNKS[k]):
             for j in range(side):
-                there = h * side + j
-
-                @pl.when(z != there)
-                def _(b=b, c=c, j=j, there=there):
-                    send(src.at[k, b * side + j], dst.at[c, z], pair(number + c), (there * nyc + yc, tp))
-
-                @pl.when(z == there)
-                def _(b=b, c=c, j=j, there=there):
-                    dst[c, there] = src[k, b * side + j]
-
-    downs.wait_recv()
-    down_all = dn[...].reshape(ntp * ff, share)
-
-    for k in range(CAP):
-        gathered[k].wait_recv()
-        hidden = hid[k].reshape(ntp * ff, experts)
-        h_yz = dot_nt(to_yz, hidden).astype(BF16)
-        ra[k] = dot(h_yz, down_all[:, :half]).astype(BF16).reshape(ra.shape[1:])
-        exchange(k, ra, ra1, yc_peers, yc, C1)
-        h_zy = dot_nt(same, hidden).astype(BF16)
-        rb[k] = dot(h_zy, down_all[:, half:]).astype(BF16).reshape(rb.shape[1:])
-        to_halves(k, rb, rb1, D1)
-
-    def forward_a(k):
-        await_all(k, ra1, yc_peers, C1)
-        reordered(k, to_zy, ra1, ra1p)
-        to_halves(k, ra1p, ra2, C2)
-
-    def forward_b(*slots):
-        for c in slots:
-            await_all(c, rb1, z_peers, D1)
-            reordered(c, to_yz, rb1, rb1p)
-            for device, there, _ in yc_peers:
-                send(rb1p.at[c, there], rb2.at[c, yc], pair(D2 + c), device)
-            rb2[c, yc] = rb1p[c, yc]
-
-    def in_half(h):
-        return lax.div(z, side) == h
-
-    for k, blocks in enumerate(CHUNKS):
-        forward_a(k)
+                to_z, first_row = h * side + j, (b * side + j) * nyc
+
+                def give(to_yc, c=c, to_z=to_z, first_row=first_row):
+                    send(leaving.at[k, first_row + to_yc], back.at[c, ep], pair(RE + c), (to_z * nyc + to_yc, tp))
+
+                pl.when(z != to_z)(functools.partial(give, yc))
+
+                @pl.when(z == to_z)
+                def _(c=c, first_row=first_row):
+                    back[c, ep] = leaving[k, first_row + yc]
+
+                for dy, dc in yc_steps:
+                    give(yc_to(dy, dc))
+
+    for step, k in ORDER:
+        if step == "down" and k == 0:
+            downs.wait_recv()
+        {"start": start_partials, "finish": finish_partials, "down": apply_down}[step](k)
+
+    sums = [0.0, 0.0]
+    for c in range(CAP):
+        everything = back.at[c, pl.ds(0, experts - 1)]
+        returns = remote(everything, everything, pair(RE + c), x_peers[0][0])
+        returns.wait_recv()
+        pending.append(returns)
+        pairs = back[c].reshape(2 * experts, half)
         for h in range(2):
-            slots = [c for c, of_half in blocks if of_half == h]
-            if slots:
-                pl.when(in_half(h))(functools.partial(forward_b, *slots))
-    for c in range(CAP):
-        for src, peers, number in ((rb, z_peers, D1), (ra1p, z_peers, C2), (rb1p, yc_peers, D2)):
-            everything = src.at[c, pl.ds(0, len(peers))]
-            pending.append(remote(everything, everything, pair(number + c), peers[0][0]))
-
-    sum_a, sum_b = 0.0, 0.0
-    for c in range(CAP):
-        await_all(c, ra2, z_peers, C2)
-        back = ra2[c].reshape(experts, half)
-        sum_a = sum_a + (dot(mix_a[c][0], back) + dot(mix_a[c][1], back))
-        await_all(c, rb2, yc_peers, D2)
-        back = rb2[c].reshape(experts, half)
-        sum_b = sum_b + (dot(mix_b[c][0], back) + dot(mix_b[c][1], back))
-    out[:, :half] = sum_a.astype(BF16)
-    out[:, half:] = sum_b.astype(BF16)
+            for part in mix[c][h]:
+                sums[h] = sums[h] + dot(part, pairs)
+    out[:, :half] = sums[0].astype(BF16)
+    out[:, half:] = sums[1].astype(BF16)
 
     for copy in pending:
         copy.wait_send()
@@ -333,13 +357,11 @@
             by_z, by_yc,
             by_yc, by_z,
             by_yc, by_z,
-            pltpu.VMEM((CAP, ntp, 2 * ff, experts), BF16),
-            pltpu.VMEM((CAP, ntp, 2 * ff, experts), BF16),
-            pltpu.VMEM((CAP, ntp, ff, experts), BF16),
-            by_yc, by_z,
-            by_yc, by_z,
-            by_z, by_yc,
-            by_z, by_yc,
+            pltpu.VMEM((NK, ntp, 2 * ff, experts), BF16),
+            pltpu.VMEM((NK, ntp, 2 * ff, experts), BF16),
+            pltpu.VMEM((NK, ntp, ff, experts), BF16),
+            pltpu.VMEM((NK, experts, 2, half), BF16),
+            pltpu.VMEM((CAP, experts, 2, half), BF16),
             dma((8,)),
             dma((DN + 1,)), dma((DN + 1,)),
         ],

time: 52 us -> 51.2 us (0.985)
  Pallas kernels: 51.2 us -> 50.4 us
    pallas_call x1, Pallas kernels: 51.2 us -> 50.4 us  [body(): pl.pallas_call(functools.partial(kernel, nz, nyc, ntp), out_shape=jax.Sha...]
where the time goes in v4:
time: 51.2 us; the launch traced here: 51.1 us
  Pallas kernels  50.4 us (98%)
  local copies, waits for them, and re-layouts  0.66 us (1%)
    pallas_call x1, Pallas kernels, body(): pl.pallas_call(functools.partial(kernel, nz, nyc, ntp), out_shape=jax.Sha...  50.4 us

profile of v4, /device:TPU:1, one launch (start us, length us, event | category | flops | bytes accessed | tf_op | source)
XLA Modules:
  0.0 51.1 jit_solution(8566334643519286571)
XLA Ops:
  0.0 50.4 %shard_map.82 = bf16[128,512]{1,0:T(8,128)(2,1)S(1)} custom-call(bf16[128,2048]{1,0:T(8,128)(2,1)} %tokens_hbm.1, f32[1,2048]{1,0:T(1,128)} %bitcast.14, s32[2,128]{1,0:T(2,128)} %bitcast.15, f32[1,128]{1,0:T(1,128)} %bitcast.17, f32[2,128]{1,0:T(2,128)} %bitcast.16, bf16[96,2048]{1,0:T(8,128)(2,1)} %bitcast.11, bf16[96,2048]{1,0:T(8,128)(2,1)} %bitcast.12, ...), custom_call_target="tpu_custom_call" | custom-call | tf_op jit(solution)/shard_map/pallas_call | solution.py:343
  50.4 0.7 %copy.10 = bf16[128,512]{1,0:T(8,128)(2,1)} copy(bf16[128,512]{1,0:T(8,128)(2,1)S(1)} %shard_map.82) | data formatting | bytes 262144

commit v5 on v4

--- a/solution.py
+++ b/solution.py
@@ -17,13 +17,13 @@
 ORDER = [
     ("start", 0),
     ("start", 1),
+    ("finish", 0),
     ("start", 2),
-    ("finish", 0),
     ("finish", 1),
     ("start", 3),
-    ("finish", 2),
     ("down", 0),
     ("down", 1),
+    ("finish", 2),
     ("finish", 3),
     ("down", 2),
     ("down", 3),

time: 51.2 us -> 50.3 us (0.982)
  Pallas kernels: 50.4 us -> 49.5 us
    pallas_call x1, Pallas kernels: 50.4 us -> 49.5 us  [body(): pl.pallas_call(functools.partial(kernel, nz, nyc, ntp), out_shape=jax.Sha...]
where the time goes in v5:
time: 50.3 us; the launch traced here: 50.1 us
  Pallas kernels  49.5 us (98%)
  local copies, waits for them, and re-layouts  0.66 us (1%)
    pallas_call x1, Pallas kernels, body(): pl.pallas_call(functools.partial(kernel, nz, nyc, ntp), out_shape=jax.Sha...  49.5 us

profile of v5, /device:TPU:1, one launch (start us, length us, event | category | flops | bytes accessed | tf_op | source)
XLA Modules:
  0.0 50.1 jit_solution(10986957794816067923)
XLA Ops:
  0.0 49.5 %shard_map.82 = bf16[128,512]{1,0:T(8,128)(2,1)S(1)} custom-call(bf16[128,2048]{1,0:T(8,128)(2,1)} %tokens_hbm.1, f32[1,2048]{1,0:T(1,128)} %bitcast.14, s32[2,128]{1,0:T(2,128)} %bitcast.15, f32[1,128]{1,0:T(1,128)} %bitcast.17, f32[2,128]{1,0:T(2,128)} %bitcast.16, bf16[96,2048]{1,0:T(8,128)(2,1)} %bitcast.11, bf16[96,2048]{1,0:T(8,128)(2,1)} %bitcast.12, ...), custom_call_target="tpu_custom_call" | custom-call | tf_op jit(solution)/shard_map/pallas_call | solution.py:343
  49.5 0.7 %copy.10 = bf16[128,512]{1,0:T(8,128)(2,1)} copy(bf16[128,512]{1,0:T(8,128)(2,1)S(1)} %shard_map.82) | data formatting | bytes 262144

commit v6 on v5

--- a/solution.py
+++ b/solution.py
@@ -167,14 +167,13 @@
 
     pl.semaphore_wait(barrier, len(z_peers) + len(yc_peers) + len(x_peers))
 
+    for device, there, d in x_peers:
+        send(gate.at[:, columns(there)], wg.at[d, pl.ds(0, ff)], pair(WG), device)
+        send(up.at[:, columns(there)], wg.at[d, pl.ds(ff, ff)], pair(WG), device)
+    gates_and_ups = remote(wg.at[others], wg.at[others], pair(WG), device)
     for c in range(CAP):
         exchange(c, oa, a1, z_peers, z, A1)
         exchange(c, ob, b1, yc_peers, yc, B1)
-        if c == 0:
-            for device, there, d in x_peers:
-                send(gate.at[:, columns(there)], wg.at[d, pl.ds(0, ff)], pair(WG), device)
-                send(up.at[:, columns(there)], wg.at[d, pl.ds(ff, ff)], pair(WG), device)
-            gates_and_ups = remote(wg.at[others], wg.at[others], pair(WG), device)
     for device, there, d in x_peers:
         send(down.at[:, columns(there)], dn.at[d], pair(DN), device)
     downs = remote(dn.at[others], dn.at[others], pair(DN), device)
@@ -292,21 +291,21 @@
             .astype(BF16)
             .reshape(n, 2, half)
         )
-        for b, (c, h) in enumerate(CHUNKS[k]):
-            for j in range(side):
-                to_z, first_row = h * side + j, (b * side + j) * nyc
-
-                def give(to_yc, c=c, to_z=to_z, first_row=first_row):
-                    send(leaving.at[k, first_row + to_yc], back.at[c, ep], pair(RE + c), (to_z * nyc + to_yc, tp))
-
-                pl.when(z != to_z)(functools.partial(give, yc))
-
-                @pl.when(z == to_z)
-                def _(c=c, first_row=first_row):
-                    back[c, ep] = leaving[k, first_row + yc]
-
-                for dy, dc in yc_steps:
-                    give(yc_to(dy, dc))
+        targets = [(h * side + j, b * side + j, c) for b, (c, h) in enumerate(CHUNKS[k]) for j in range(side)]
+        for to_z, group, c in sorted(targets):
+            first_row = group * nyc
+
+            def give(to_yc, c=c, to_z=to_z, first_row=first_row):
+                send(leaving.at[k, first_row + to_yc], back.at[c, ep], pair(RE + c), (to_z * nyc + to_yc, tp))
+
+            pl.when(z != to_z)(functools.partial(give, yc))
+
+            @pl.when(z == to_z)
+            def _(c=c, first_row=first_row):
+                back[c, ep] = leaving[k, first_row + yc]
+
+            for dy, dc in yc_steps:
+                give(yc_to(dy, dc))
 
     for step, k in ORDER:
         if step == "down" and k == 0:

time: 50.3 us -> 50.2 us (level)
  no operation moved by 1% of the time
where the time goes in v6:
time: 50.2 us; the launch traced here: 50.1 us
  Pallas kernels  49.4 us (98%)
  local copies, waits for them, and re-layouts  0.66 us (1%)
    pallas_call x1, Pallas kernels, body(): pl.pallas_call(functools.partial(kernel, nz, nyc, ntp), out_shape=jax.Sha...  49.4 us

profile of v6, /device:TPU:1, one launch (start us, length us, event | category | flops | bytes accessed | tf_op | source)
XLA Modules:
  0.0 50.1 jit_solution(1101460759926313185)
XLA Ops:
  0.0 49.4 %shard_map.82 = bf16[128,512]{1,0:T(8,128)(2,1)S(1)} custom-call(bf16[128,2048]{1,0:T(8,128)(2,1)} %tokens_hbm.1, f32[1,2048]{1,0:T(1,128)} %bitcast.14, s32[2,128]{1,0:T(2,128)} %bitcast.15, f32[1,128]{1,0:T(1,128)} %bitcast.17, f32[2,128]{1,0:T(2,128)} %bitcast.16, bf16[96,2048]{1,0:T(8,128)(2,1)} %bitcast.11, bf16[96,2048]{1,0:T(8,128)(2,1)} %bitcast.12, ...), custom_call_target="tpu_custom_call" | custom-call | tf_op jit(solution)/shard_map/pallas_call | solution.py:342
  49.5 0.7 %copy.10 = bf16[128,512]{1,0:T(8,128)(2,1)} copy(bf16[128,512]{1,0:T(8,128)(2,1)S(1)} %shard_map.82) | data formatting | bytes 262144
